TPU v7x, 32 devices: a whole 2x2x4 slice. The times are simulated.
32 devices in a mesh: fs: 8 (over z, y), tp: 4 (over x, core).
Axes of the slice: x: 2, y: 2, z: 4, core: 2. Of those that a mesh axis runs over, the one named last changes fastest.
Arguments:
- inputs: bfloat16 [4608, 2048], P('fs'), may hold values from -6 to 6
- query_cotangent: bfloat16 [4608, 1024], P('fs', 'tp'), may hold values from -0.017944336 to 0.017944336
- value_cotangent: bfloat16 [4608, 1024], P('fs', 'tp'), may hold values from -0.017944336 to 0.017944336
- weights_query: float32 [2048, 1024], P('fs', 'tp'), may hold values from -6 to 6
- weights_value: float32 [2048, 1024], P('fs', 'tp'), may hold values from -6 to 6
- basis_query: bfloat16 [1024, 32], P('tp'), may hold values from -0.75 to 0.75
- basis_value: bfloat16 [1024, 32], P('tp'), may hold values from -0.75 to 0.75
- first_query: float32 [2048, 512], P('fs', 'tp'), may hold values from -5.4 to 5.4, as said below
- second_query: float32 [2048, 512], P('fs', 'tp'), may hold values from 0.05 to 1
- first_value: float32 [2048, 512], P('fs', 'tp'), may hold values from -5.4 to 5.4, as said below
- second_value: float32 [2048, 512], P('fs', 'tp'), may hold values from 0.05 to 1
Outputs:
- step_query: float32 [2048, 1024], P('fs', 'tp')
- step_value: float32 [2048, 1024], P('fs', 'tp')
- new_query: float32 [2048, 1024], P('fs', 'tp')
- new_value: float32 [2048, 1024], P('fs', 'tp')
- copy_query: bfloat16 [2048, 1024], P(None, 'tp')
- copy_value: bfloat16 [2048, 1024], P(None, 'tp')
- moment_query: float32 [2048, 512], P('fs', 'tp')
- square_query: float32 [2048, 512], P('fs', 'tp')
- moment_value: float32 [2048, 512], P('fs', 'tp')
- square_value: float32 [2048, 512], P('fs', 'tp')
Inputs may be any that keep to these rules, and one draw needn't show every extreme that they name: `first_query`: first moments, with a spread of scale from row to row. `first_value`: first moments, with a spread of scale from row to row.
All inputs are finite; a program needn't handle non-finite values.
Results may differ from a plain program's by a relative error of at most 0.003.
Values may be sent and summed in bfloat16 or wider, within the bound.
A program may use at most 64 MiB of HBM per device.

v0:
```python
import jax
import jax.numpy as jnp
from jax import lax
from jax.sharding import PartitionSpec as P

D = 2048
HEADS = 16
HEAD = 64
RK = 32


def from_space(direction, factor, heads_here):
    count = direction.shape[0]
    split = direction.reshape(count, heads_here, RK)
    out = jnp.einsum("nhr,hdr->nhd", split, factor, precision=lax.Precision.HIGHEST)
    return out.reshape(count, heads_here * HEAD)


def moments(reduced, first, second):
    moment = 0.9 * first + 0.1 * reduced
    square = 0.95 * second + 0.05 * reduced * reduced
    direction = moment / (jnp.sqrt(square) + 1e-08)
    return (moment, square, direction)


def per_device(
    inputs,
    query_cotangent,
    value_cotangent,
    weights_query,
    weights_value,
    basis_query,
    basis_value,
    first_query,
    second_query,
    first_value,
    second_value,
):
    own_cols = weights_query.shape[1]
    heads_here = own_cols // HEAD
    space_cols = heads_here * RK
    factor_q = basis_query.reshape(heads_here, HEAD, RK).astype(jnp.float32)
    factor_v = basis_value.reshape(heads_here, HEAD, RK).astype(jnp.float32)
    contract = (((0,), (0,)), ((), ()))
    tok_count = query_cotangent.shape[0]
    bf_q = basis_query.reshape(heads_here, HEAD, RK)
    bf_v = basis_value.reshape(heads_here, HEAD, RK)
    small_q = jnp.einsum(
        "thd,hdr->thr",
        query_cotangent.reshape(tok_count, heads_here, HEAD),
        bf_q,
        preferred_element_type=jnp.float32,
    )
    small_v = jnp.einsum(
        "thd,hdr->thr",
        value_cotangent.reshape(tok_count, heads_here, HEAD),
        bf_v,
        preferred_element_type=jnp.float32,
    )
    small_both = jnp.concatenate(
        (small_q.reshape(tok_count, space_cols), small_v.reshape(tok_count, space_cols)), axis=1
    )
    upper_part = small_both.astype(jnp.bfloat16)
    lower_part = (small_both - upper_part.astype(jnp.float32)).astype(jnp.bfloat16)
    high = lax.dot_general(inputs, upper_part, contract, preferred_element_type=jnp.float32)
    reduced = lax.psum_scatter(
        high + lax.dot_general(inputs, lower_part, contract, preferred_element_type=jnp.float32),
        "fs",
        scatter_dimension=0,
        tiled=True,
    )
    reduced_q = reduced[:, :space_cols]
    reduced_v = reduced[:, space_cols:]
    moment_q, square_q, direction_q = moments(reduced_q, first_query, second_query)
    moment_v, square_v, direction_v = moments(reduced_v, first_value, second_value)
    total_q, total_v = lax.psum(
        (jnp.sum(direction_q * direction_q), jnp.sum(direction_v * direction_v)), ("fs", "tp")
    )
    entries = D * HEADS * RK
    scale_q = 1.0 / jnp.sqrt(total_q / entries + 0.25)
    scale_v = 1.0 / jnp.sqrt(total_v / entries + 0.25)
    step_q = scale_q * from_space(direction_q, factor_q, heads_here)
    step_v = scale_v * from_space(direction_v, factor_v, heads_here)
    fresh_q = weights_query - 0.1 * step_q
    fresh_v = weights_value - 0.1 * step_v
    copy_q, copy_v = (
        lax.all_gather(fresh_q.astype(jnp.bfloat16), "fs", axis=0, tiled=True),
        lax.all_gather(fresh_v.astype(jnp.bfloat16), "fs", axis=0, tiled=True),
    )
    return (
        step_q,
        step_v,
        fresh_q,
        fresh_v,
        copy_q,
        copy_v,
        moment_q,
        square_q,
        moment_v,
        square_v,
    )


def solution(mesh):
    placed = (
        P("fs", None),
        P("fs", "tp"),
        P("fs", "tp"),
        P("fs", "tp"),
        P("fs", "tp"),
        P("tp", None),
        P("tp", None),
        P("fs", "tp"),
        P("fs", "tp"),
        P("fs", "tp"),
        P("fs", "tp"),
    )
    return jax.shard_map(
        per_device,
        mesh=mesh,
        in_specs=placed,
        out_specs=(
            P("fs", "tp"),
            P("fs", "tp"),
            P("fs", "tp"),
            P("fs", "tp"),
            P(None, "tp"),
            P(None, "tp"),
            P("fs", "tp"),
            P("fs", "tp"),
            P("fs", "tp"),
            P("fs", "tp"),
        ),
        check_vma=False,
    )
```

profile of v0, /device:TPU:0, one launch (start us, length us, event | category | flops | bytes accessed | tf_op | source)
XLA Modules:
  0.0 223.8 jit_solution(16746739006652718097)
XLA Ops:
  7.2 1.0 reshape.52
  8.2 0.8 reshape.55
  9.0 1.2 copy.40
  10.2 1.2 copy.42
  11.4 0.2 fusion.10
  11.6 0.2 fusion.7
  11.8 1.0 fusion.2
  12.8 2.3 %fusion = f32[2048,256]{0,1:T(8,128)} fusion(f32[256,2048]{1,0:T(8,128)S(1)} %fusion.2, bf16[576,2048]{1,0:T(8,128)(2,1)S(1)} %copy-done, f32[576,128]{0,1:T(8,128)S(1)} %bitcast.31, f32[576,128]{0,1:T(8,128)S(1)} %bitcast.29), kind=kOutput, calls=%fused_computation.1 | convolution fusion | flops 605241344 | bytes 7143424 | tf_op jit(solution)/shard_map/dot_general | solution.py:67
  15.2 0.0 all-gather.5.cloned.1.call-start
  15.2 0.1 copy.39
  15.3 0.7 copy-done.6
  16.0 0.1 copy.44
  16.1 0.1 copy.46
  16.3 0.1 copy.47
  16.4 70.6 %reduce-scatter.2.cloned.1.call-done = f32[256,256]{0,1:T(8,128)} async-done(((f32[2048,256]{0,1:T(8,128)}), f32[256,256]{0,1:T(8,128)}) %reduce-scatter.2.cloned.1.call-update) | async-done | bytes 262160 | tf_op jit(solution)/shard_map/reduce_scatter | solution.py:66
  86.9 2.4 %multiply_reduce_fusion = (f32[]{:T(128)}, f32[256,128]{0,1:T(8,128)S(1)}, f32[256,128]{0,1:T(8,128)}, f32[256,128]{0,1:T(8,128)S(1)}, f32[]{:T(128)}, /*index=5...) fusion(f32[256,256]{0,1:T(8,128)} %reduce-scatter.2.cloned.1.call-done, f32[256,128]{0,1:T(8,128)S(1)} %copy.47, ...), kind=kLoop, calls=%fused_computation.14 | loop fusion | flops 720894 | bytes 1572872 | tf_op jit(solution)/shard_map/reduce_sum | solution.py:77
  89.3 39.8 %all-reduce = (f32[]{:T(128)}, f32[]{:T(128)}) all-reduce(f32[]{:T(128)} %get-tuple-element.44, f32[]{:T(128)} %get-tuple-element.36), channel_id=1, replica_groups=mesh['fs'=8,'tp'=4] {'fs','tp'}, use_global_device_ids=true, to_apply=%region_2.0 | all-reduce | flops 2 | bytes 16 | tf_op jit(solution)/shard_map/psum | solution.py:76
  129.8 0.3 convolution_multiply_fusion
  130.1 0.1 copy.52
  130.3 1.8 fusion.14
  132.1 0.0 all-gather.3.cloned.1.call-start
  132.9 1.2 convolution_multiply_fusion.1
  134.1 0.1 copy.51
  134.2 1.8 fusion.15
  136.1 1.7 copy.56
  137.8 0.8 copy.55
  138.5 0.8 copy.54
  139.3 0.8 copy.53
  140.0 32.2 %all-gather.5.cloned.1.call-done = bf16[2048,256]{1,0:T(8,128)(2,1)} async-done(((bf16[256,256]{1,0:T(8,128)(2,1)}), bf16[2048,256]{1,0:T(8,128)(2,1)}) %all-gather.5.cloned.1.call-update) | async-done | bytes 1048592 | tf_op jit(solution)/shard_map/all_gather | solution.py:88
  172.3 41.7 %all-gather.3.cloned.1.call-done = bf16[2048,256]{1,0:T(8,128)(2,1)} async-done(((bf16[256,256]{1,0:T(8,128)(2,1)}), bf16[2048,256]{1,0:T(8,128)(2,1)}) %all-gather.3.cloned.1.call-update) | async-done | bytes 1048592 | tf_op jit(solution)/shard_map/all_gather | solution.py:87
  214.0 2.4 %copy.67 = bf16[2048,256]{1,0:T(8,128)(2,1)} copy(bf16[2048,256]{1,0:T(8,128)(2,1)} %all-gather.3.cloned.1.call-done) | data formatting | bytes 2097152
  216.3 1.0 copy.68
  (21 shorter events, 0.1 us)
Async XLA Ops:
  7.2 4.6 %copy-start = (bf16[576,2048]{1,0:T(8,128)(2,1)S(1)}, bf16[576,2048]{1,0:T(8,128)(2,1)}, u32[]{:S(2)}) copy-start(bf16[576,2048]{1,0:T(8,128)(2,1)} %param.11) | copy-start | bytes 7077892
  7.2 79.7 %reduce-scatter.2.cloned.1.call-start = ((), (), s32[]{:S(2)}) async-start(), calls=%async_computation.1 | async-start | bytes 2359296 | tf_op jit(solution)/shard_map/reduce_scatter | solution.py:66
  8.2 4.6 %copy-start.4 = (bf16[4,64,32]{1,0,2:T(4,128)(2,1)}, bf16[4,64,32]{1,0,2:T(4,128)(2,1)S(1)}, u32[]{:S(2)}) copy-start(bf16[4,64,32]{1,0,2:T(4,128)(2,1)S(1)} %reshape.52) | copy-start | bytes 49156
  12.8 2.4 %copy-start.5 = (f32[256,128]{1,0:T(8,128)S(1)}, f32[256,128]{1,0:T(8,128)}, u32[]{:S(2)}) copy-start(f32[256,128]{1,0:T(8,128)} %param.18) | copy-start | bytes 393220
  15.1 0.9 copy-start.6
  15.1 1.0 copy-start.7
  15.1 1.1 copy-start.8
  15.2 157.1 %all-gather.5.cloned.1.call-start = ((), (), s32[]{:S(2)}) async-start(), calls=%async_computation.3 | async-start | bytes 1179648 | tf_op jit(solution)/shard_map/all_gather | solution.py:88
  130.3 86.1 %copy-start.1 = (f32[256,256]{1,0:T(8,128)}, f32[256,256]{1,0:T(8,128)S(1)}, u32[]{:S(2)}) copy-start(f32[256,256]{1,0:T(8,128)S(1)} %copy.52) | copy-start | bytes 786436
  132.1 81.8 %all-gather.3.cloned.1.call-start = ((), (), s32[]{:S(2)}) async-start(), calls=%async_computation.2 | async-start | bytes 1179648 | tf_op jit(solution)/shard_map/all_gather | solution.py:87
  134.2 83.1 %copy-start.2 = (f32[256,256]{1,0:T(8,128)}, f32[256,256]{1,0:T(8,128)S(1)}, u32[]{:S(2)}) copy-start(f32[256,256]{1,0:T(8,128)S(1)} %copy.51) | copy-start | bytes 786436
  214.0 2.4 %copy-start.3 = (bf16[2048,256]{1,0:T(8,128)(2,1)S(1)}, bf16[2048,256]{1,0:T(8,128)(2,1)}, u32[]{:S(2)}) copy-start(bf16[2048,256]{1,0:T(8,128)(2,1)} %all-gather.5.cloned.1.call-done) | copy-start | bytes 3145732
Sparse Core Ops, SparseCore 0:
  15.3 71.6 reduce-scatter.1
  132.3 39.9 all-gather.4
  175.0 38.9 all-gather.2
where the time goes:
time: 224 us
  waiting for transfers between devices  145 us (65%)
  blocking collectives  39.8 us (18%)
  between operations  15.3 us (7%)
  local copies, waits for them, and re-layouts  12.7 us (6%)
  other arithmetic  6.06 us (3%)
  matrix products  5.25 us (2%)
    reduce_scatter x1, waiting for transfers between devices, per_device(): lax.psum_scatter(high + lax.dot_general(inputs, lower_part, contract, pre...  70.6 us
    all_gather x1, waiting for transfers between devices, per_device(): lax.all_gather(fresh_q.astype(jnp.bfloat16), 'fs', axis=0, tiled=True)  41.7 us
    psum x1, blocking collectives, per_device(): lax.psum((jnp.sum(direction_q * direction_q), jnp.sum(direction_v * direc...  39.8 us
    all_gather x1, waiting for transfers between devices, per_device(): lax.all_gather(fresh_v.astype(jnp.bfloat16), 'fs', axis=0, tiled=True)  32.2 us
    unnamed x32, local copies, waits for them, and re-layouts  11 us
  transfers between devices with their start and end apart: 3, of which 3 were waited for; matrix products, arithmetic and copies ran while one was open for 3% of the time, Pallas kernels for 0%

commit v1 on v0

--- a/solution.py
+++ b/solution.py
@@ -1,3 +1,4 @@
+import functools
 import jax
 import jax.numpy as jnp
 from jax import lax
@@ -7,6 +8,31 @@
 HEADS = 16
 HEAD = 64
 RK = 32
+
+
+def turn_digits(buf, mesh_ax):
+    near = lax.axis_size(mesh_ax)
+    heard, f_next, last = (near, lax.axis_index(mesh_ax), buf.shape[0])
+    fields = tuple((to_i * heard if k == 0 else to_i for k, to_i in enumerate(buf.shape)))
+    before = jnp.zeros(fields, buf.dtype)
+    carry_in = lax.dynamic_update_slice_in_dim(before, buf, f_next * last, axis=0)
+    val = g_now = buf
+    for dd in range(1, heard // 2 + 1):
+        val = lax.ppermute(val, mesh_ax, tuple(((k, (k + 1) % heard) for k in range(heard))))
+        carry_in = lax.dynamic_update_slice_in_dim(
+            carry_in, val, (f_next - dd) % heard * last, axis=0
+        )
+        if 2 * dd < heard:
+            g_now = lax.ppermute(
+                g_now, mesh_ax, tuple(((k, (k - 1) % heard) for k in range(heard)))
+            )
+            carry_in = lax.dynamic_update_slice_in_dim(
+                carry_in, g_now, (f_next + dd) % heard * last, axis=0
+            )
+    return carry_in
+
+
+object_make = functools.partial(turn_digits, mesh_ax="fs")
 
 
 def from_space(direction, factor, heads_here):
@@ -84,7 +110,7 @@
     fresh_q = weights_query - 0.1 * step_q
     fresh_v = weights_value - 0.1 * step_v
     copy_q, copy_v = (
-        lax.all_gather(fresh_q.astype(jnp.bfloat16), "fs", axis=0, tiled=True),
+        object_make(fresh_q.astype(jnp.bfloat16)),
         lax.all_gather(fresh_v.astype(jnp.bfloat16), "fs", axis=0, tiled=True),
     )
     return (

time: 224 us -> 188 us (0.84)
  waiting for transfers between devices: 145 us -> 88.2 us
  starting transfers between devices: 0.12 us -> 14.2 us
  local copies, waits for them, and re-layouts: 12.7 us -> 17.4 us
    all_gather x1 -> x0, waiting for transfers between devices: 41.7 us -> none  [per_device(): lax.all_gather(fresh_q.astype(jnp.bfloat16), 'fs', axis=0, tiled=True)]
    all_gather x1, waiting for transfers between devices: 32.2 us -> 5.64 us  [per_device(): lax.all_gather(fresh_v.astype(jnp.bfloat16), 'fs', axis=0, tiled=True)]
    ppermute x0 -> x7, starting transfers between devices: none -> 14.1 us  [the longest x3 9.02 us: turn_digits(): lax.ppermute(g_now, mesh_ax, tuple(((k, (k - 1) % heard) for k in range(h...]
    ppermute x0 -> x7, waiting for transfers between devices: none -> 11.9 us  [the longest x4 10.3 us: turn_digits(): lax.ppermute(val, mesh_ax, tuple(((k, (k + 1) % heard) for k in range(hea...]
    dynamic_update_slice x0 -> x7, local copies, waits for them, and re-layouts: none -> 5.55 us  [the longest x4 3.56 us: turn_digits(): lax.dynamic_update_slice_in_dim(carry_in, val, (f_next - dd) % heard * la...]
    unnamed x32 -> x33, local copies, waits for them, and re-layouts: 11 us -> 9.01 us
  transfers between devices with their start and end apart: 3 -> 9, of which waited for: 3 -> 8; matrix products, arithmetic and copies ran while one was open for 3% -> 7% of each run, Pallas kernels for 0% -> 0%
where the time goes in v1:
time: 188 us; the launch traced here: 187 us
  waiting for transfers between devices  88.2 us (47%)
  blocking collectives  39.8 us (21%)
  local copies, waits for them, and re-layouts  17.4 us (9%)
  between operations  15.6 us (8%)
  starting transfers between devices  14.2 us (8%)
  other arithmetic  5.96 us (3%)
  matrix products  5.85 us (3%)
    reduce_scatter x1, waiting for transfers between devices, per_device(): lax.psum_scatter(high + lax.dot_general(inputs, lower_part, contract, pre...  70.6 us
    psum x1, blocking collectives, per_device(): lax.psum((jnp.sum(direction_q * direction_q), jnp.sum(direction_v * direc...  39.8 us
    ppermute x4, waiting for transfers between devices, turn_digits(): lax.ppermute(val, mesh_ax, tuple(((k, (k + 1) % heard) for k in range(hea...  10.3 us
    ppermute x3, starting transfers between devices, turn_digits(): lax.ppermute(g_now, mesh_ax, tuple(((k, (k - 1) % heard) for k in range(h...  9.02 us
    unnamed x33, local copies, waits for them, and re-layouts  9.01 us
    all_gather x1, waiting for transfers between devices, per_device(): lax.all_gather(fresh_v.astype(jnp.bfloat16), 'fs', axis=0, tiled=True)  5.64 us
    ppermute x4, starting transfers between devices, turn_digits(): lax.ppermute(val, mesh_ax, tuple(((k, (k + 1) % heard) for k in range(hea...  5.09 us
  transfers between devices with their start and end apart: 9, of which 8 were waited for; matrix products, arithmetic and copies ran while one was open for 7% of the time, Pallas kernels for 0%

profile of v1, /device:TPU:0, one launch (start us, length us, event | category | flops | bytes accessed | tf_op | source)
XLA Modules:
  0.0 187.0 jit_solution(2433859172806822182)
XLA Ops:
  7.2 1.0 reshape.52
  8.2 0.8 reshape.55
  9.0 1.2 copy.40
  10.2 1.2 copy.42
  11.8 1.0 fusion.2
  12.8 2.3 %fusion = f32[2048,256]{0,1:T(8,128)} fusion(f32[256,2048]{1,0:T(8,128)S(1)} %fusion.2, bf16[576,2048]{1,0:T(8,128)(2,1)S(1)} %copy-done, f32[576,128]{0,1:T(8,128)S(1)} %bitcast.31, f32[576,128]{0,1:T(8,128)S(1)} %bitcast.29), kind=kOutput, calls=%fused_computation.1 | convolution fusion | flops 605241344 | bytes 7143424 | tf_op jit(solution)/shard_map/dot_general | solution.py:93
  15.4 0.7 copy-done.7
  16.4 70.6 %reduce-scatter.2.cloned.1.call-done = f32[256,256]{0,1:T(8,128)} async-done(((f32[2048,256]{0,1:T(8,128)}), f32[256,256]{0,1:T(8,128)}) %reduce-scatter.2.cloned.1.call-update) | async-done | bytes 262160 | tf_op jit(solution)/shard_map/reduce_scatter | solution.py:92
  86.9 2.4 %multiply_reduce_fusion = (f32[]{:T(128)}, f32[256,128]{0,1:T(8,128)S(1)}, f32[256,128]{0,1:T(8,128)}, f32[256,128]{0,1:T(8,128)S(1)}, f32[]{:T(128)}, /*index=5...) fusion(f32[256,256]{0,1:T(8,128)} %reduce-scatter.2.cloned.1.call-done, f32[256,128]{0,1:T(8,128)S(1)} %copy.47, ...), kind=kLoop, calls=%fused_computation.14 | loop fusion | flops 720894 | bytes 1572872 | tf_op jit(solution)/shard_map/reduce_sum | solution.py:103
  89.3 39.8 %all-reduce = (f32[]{:T(128)}, f32[]{:T(128)}) all-reduce(f32[]{:T(128)} %get-tuple-element.45, f32[]{:T(128)} %get-tuple-element.37), channel_id=1, replica_groups=mesh['fs'=8,'tp'=4] {'fs','tp'}, use_global_device_ids=true, to_apply=%region_2.0 | all-reduce | flops 2 | bytes 16 | tf_op jit(solution)/shard_map/psum | solution.py:102
  129.8 1.1 convolution_multiply_fusion
  131.0 1.8 fusion.14
  133.6 1.1 convolution_multiply_fusion.1
  134.8 1.0 broadcast_in_dim.3
  135.8 1.8 constant_dynamic-update-slice_fusion.7
  137.6 2.5 %collective-permute-start = (bf16[256,256]{1,0:T(8,128)(2,1)}, bf16[256,256]{1,0:T(8,128)(2,1)}, u32[]{:S(2)}, u32[]{:S(2)}) collective-permute-start(bf16[256,256]{1,0:T(8,128)(2,1)} %get-tuple-element.35), channel_id=1, source_target_pairs={{0,4},{4,8},{8,12},{12,16},{16,20},{20,24},{24,28},{28,0},{1,5},{5... | collective-permute-start | bytes 393224 | tf_op jit(solution)/shard_map/ppermute | solution.py:21
  140.1 2.3 %collective-permute-start.1 = (bf16[256,256]{1,0:T(8,128)(2,1)}, bf16[256,256]{1,0:T(8,128)(2,1)S(1)}, u32[]{:S(2)}, u32[]{:S(2)}) collective-permute-start(bf16[256,256]{1,0:T(8,128)(2,1)} %get-tuple-element.35), channel_id=1, source_target_pairs={{0,28},{4,0},{8,4},{12,8},{16,12},{20,16},{24,20},{28,24},{1,29},{... | collective-permute-start | bytes 393224 | tf_op jit(solution)/shard_map/ppermute | solution.py:26
  142.3 0.8 copy.56
  143.1 0.8 copy.55
  143.8 0.8 copy.54
  144.6 0.8 copy.53
  145.8 2.6 %collective-permute-start.2 = (bf16[256,256]{1,0:T(8,128)(2,1)}, bf16[256,256]{1,0:T(8,128)(2,1)S(1)}, u32[]{:S(2)}, u32[]{:S(2)}) collective-permute-start(bf16[256,256]{1,0:T(8,128)(2,1)} %collective-permute-done), channel_id=1, source_target_pairs={{0,4},{4,8},{8,12},{12,16},{16,20},{20,24},{24,28},{28,0},{1,5},{5... | collective-permute-start | bytes 393224 | tf_op jit(solution)/shard_map/ppermute | solution.py:21
  148.6 2.0 %collective-permute-start.3 = (bf16[256,256]{1,0:T(8,128)(2,1)S(1)}, bf16[256,256]{1,0:T(8,128)(2,1)S(1)}, u32[]{:S(2)}, u32[]{:S(2)}) collective-permute-start(bf16[256,256]{1,0:T(8,128)(2,1)S(1)} %collective-permute-done.1), channel_id=1, source_target_pairs={{0,28},{4,0},{8,4},{12,8},{16,12},{20,16},{24,20},{28,24},{1,29},{... | collective-permute-start | bytes 393224 | tf_op jit(solution)/shard_map/ppermute | solution.py:26
  150.6 1.6 constant_dynamic-update-slice_fusion.6
  152.9 2.8 %collective-permute-done.2 = bf16[256,256]{1,0:T(8,128)(2,1)S(1)} collective-permute-done((bf16[256,256]{1,0:T(8,128)(2,1)}, bf16[256,256]{1,0:T(8,128)(2,1)S(1)}, u32[]{:S(2)}, u32[]{:S(2)}) %collective-permute-start.2) | collective-permute-done | bytes 131104 | tf_op jit(solution)/shard_map/ppermute | solution.py:21
  155.7 4.7 %collective-permute-start.5 = (bf16[256,256]{1,0:T(8,128)(2,1)S(1)}, bf16[256,256]{1,0:T(8,128)(2,1)S(1)}, u32[]{:S(2)}, u32[]{:S(2)}) collective-permute-start(bf16[256,256]{1,0:T(8,128)(2,1)S(1)} %collective-permute-done.3), channel_id=1, source_target_pairs={{0,28},{4,0},{8,4},{12,8},{16,12},{20,16},{24,20},{28,24},{1,29},{... | collective-permute-start | bytes 393224 | tf_op jit(solution)/shard_map/ppermute | solution.py:26
  161.7 1.6 collective-permute-done.4
  163.4 0.7 constant_dynamic-update-slice_fusion.2
  164.0 1.5 collective-permute-done.5
  166.2 5.4 %collective-permute-done.6 = bf16[256,256]{1,0:T(8,128)(2,1)S(1)} collective-permute-done((bf16[256,256]{1,0:T(8,128)(2,1)S(1)}, bf16[256,256]{1,0:T(8,128)(2,1)S(1)}, u32[]{:S(2)}, u32[]{:S(2)}) %collective-permute-start.6) | collective-permute-done | bytes 131104 | tf_op jit(solution)/shard_map/ppermute | solution.py:21
  172.2 5.6 %all-gather.2.cloned.1.call-done = bf16[2048,256]{1,0:T(8,128)(2,1)} async-done(((bf16[256,256]{1,0:T(8,128)(2,1)}), bf16[2048,256]{1,0:T(8,128)(2,1)}) %all-gather.2.cloned.1.call-update) | async-done | bytes 1048592 | tf_op jit(solution)/shard_map/all_gather | solution.py:114
  177.9 2.3 %copy.74 = bf16[2048,256]{1,0:T(8,128)(2,1)} copy(bf16[2048,256]{1,0:T(8,128)(2,1)} %all-gather.2.cloned.1.call-done) | data formatting | bytes 2097152
  (41 shorter events, 5.1 us)
Async XLA Ops:
  7.2 4.6 %copy-start = (bf16[576,2048]{1,0:T(8,128)(2,1)S(1)}, bf16[576,2048]{1,0:T(8,128)(2,1)}, u32[]{:S(2)}) copy-start(bf16[576,2048]{1,0:T(8,128)(2,1)} %param.11) | copy-start | bytes 7077892
  7.2 79.7 %reduce-scatter.2.cloned.1.call-start = ((), (), s32[]{:S(2)}) async-start(), calls=%async_computation.1 | async-start | bytes 2359296 | tf_op jit(solution)/shard_map/reduce_scatter | solution.py:92
  8.2 6.9 %copy-start.4 = (bf16[4,64,32]{1,0,2:T(4,128)(2,1)}, bf16[4,64,32]{1,0,2:T(4,128)(2,1)S(1)}, u32[]{:S(2)}) copy-start(bf16[4,64,32]{1,0,2:T(4,128)(2,1)S(1)} %reshape.52) | copy-start | bytes 49156
  9.0 6.1 %copy-start.5 = (bf16[4,64,32]{1,0,2:T(4,128)(2,1)}, bf16[4,64,32]{1,0,2:T(4,128)(2,1)S(1)}, u32[]{:S(2)}) copy-start(bf16[4,64,32]{1,0,2:T(4,128)(2,1)S(1)} %reshape.55) | copy-start | bytes 49156
  12.8 2.5 %copy-start.6 = (f32[256,128]{1,0:T(8,128)S(1)}, f32[256,128]{1,0:T(8,128)}, u32[]{:S(2)}) copy-start(f32[256,128]{1,0:T(8,128)} %param.18) | copy-start | bytes 393220
  15.1 0.9 copy-start.7
  15.1 1.0 copy-start.8
  15.2 1.1 copy-start.9
  15.2 162.7 %all-gather.2.cloned.1.call-start = ((), (), s32[]{:S(2)}) async-start(), calls=%async_computation.2 | async-start | bytes 1179648 | tf_op jit(solution)/shard_map/all_gather | solution.py:114
  131.0 12.8 %copy-start.1 = (f32[256,256]{1,0:T(8,128)}, f32[256,256]{1,0:T(8,128)S(1)}, u32[]{:S(2)}) copy-start(f32[256,256]{1,0:T(8,128)S(1)} %copy.52) | copy-start | bytes 786436
  134.8 31.4 %copy-start.2 = (f32[256,256]{1,0:T(8,128)}, f32[256,256]{1,0:T(8,128)S(1)}, u32[]{:S(2)}) copy-start(f32[256,256]{1,0:T(8,128)S(1)} %copy.51) | copy-start | bytes 786436
  134.8 7.6 %copy-start.3 = (f32[256,128]{0,1:T(8,128)S(1)}, f32[256,128]{0,1:T(8,128)}, u32[]{:S(2)}) copy-start(f32[256,128]{0,1:T(8,128)} %get-tuple-element.39) | copy-start | bytes 393220
  137.6 8.2 %collective-permute-start = (bf16[256,256]{1,0:T(8,128)(2,1)}, bf16[256,256]{1,0:T(8,128)(2,1)}, u32[]{:S(2)}, u32[]{:S(2)}) collective-permute-start(bf16[256,256]{1,0:T(8,128)(2,1)} %get-tuple-element.35), channel_id=1, source_target_pairs={{0,4},{4,8},{8,12},{12,16},{16,20},{20,24},{24,28},{28,0},{1,5},{5... | collective-permute-start | bytes 393224 | tf_op jit(solution)/shard_map/ppermute | solution.py:21
  140.1 8.5 %collective-permute-start.1 = (bf16[256,256]{1,0:T(8,128)(2,1)}, bf16[256,256]{1,0:T(8,128)(2,1)S(1)}, u32[]{:S(2)}, u32[]{:S(2)}) collective-permute-start(bf16[256,256]{1,0:T(8,128)(2,1)} %get-tuple-element.35), channel_id=1, source_target_pairs={{0,28},{4,0},{8,4},{12,8},{16,12},{20,16},{24,20},{28,24},{1,29},{... | collective-permute-start | bytes 393224 | tf_op jit(solution)/shard_map/ppermute | solution.py:26
  145.8 9.8 %collective-permute-start.2 = (bf16[256,256]{1,0:T(8,128)(2,1)}, bf16[256,256]{1,0:T(8,128)(2,1)S(1)}, u32[]{:S(2)}, u32[]{:S(2)}) collective-permute-start(bf16[256,256]{1,0:T(8,128)(2,1)} %collective-permute-done), channel_id=1, source_target_pairs={{0,4},{4,8},{8,12},{12,16},{16,20},{20,24},{24,28},{28,0},{1,5},{5... | collective-permute-start | bytes 393224 | tf_op jit(solution)/shard_map/ppermute | solution.py:21
  148.6 7.1 %collective-permute-start.3 = (bf16[256,256]{1,0:T(8,128)(2,1)S(1)}, bf16[256,256]{1,0:T(8,128)(2,1)S(1)}, u32[]{:S(2)}, u32[]{:S(2)}) collective-permute-start(bf16[256,256]{1,0:T(8,128)(2,1)S(1)} %collective-permute-done.1), channel_id=1, source_target_pairs={{0,28},{4,0},{8,4},{12,8},{16,12},{20,16},{24,20},{28,24},{1,29},{... | collective-permute-start | bytes 393224 | tf_op jit(solution)/shard_map/ppermute | solution.py:26
  155.7 7.7 %collective-permute-start.4 = (bf16[256,256]{1,0:T(8,128)(2,1)S(1)}, bf16[256,256]{1,0:T(8,128)(2,1)S(1)}, u32[]{:S(2)}, u32[]{:S(2)}) collective-permute-start(bf16[256,256]{1,0:T(8,128)(2,1)S(1)} %collective-permute-done.2), channel_id=1, source_target_pairs={{0,4},{4,8},{8,12},{12,16},{16,20},{20,24},{24,28},{28,0},{1,5},{5... | collective-permute-start | bytes 393224 | tf_op jit(solution)/shard_map/ppermute | solution.py:21
  155.7 9.8 %collective-permute-start.5 = (bf16[256,256]{1,0:T(8,128)(2,1)S(1)}, bf16[256,256]{1,0:T(8,128)(2,1)S(1)}, u32[]{:S(2)}, u32[]{:S(2)}) collective-permute-start(bf16[256,256]{1,0:T(8,128)(2,1)S(1)} %collective-permute-done.3), channel_id=1, source_target_pairs={{0,28},{4,0},{8,4},{12,8},{16,12},{20,16},{24,20},{28,24},{1,29},{... | collective-permute-start | bytes 393224 | tf_op jit(solution)/shard_map/ppermute | solution.py:26
  163.4 8.2 %collective-permute-start.6 = (bf16[256,256]{1,0:T(8,128)(2,1)S(1)}, bf16[256,256]{1,0:T(8,128)(2,1)S(1)}, u32[]{:S(2)}, u32[]{:S(2)}) collective-permute-start(bf16[256,256]{1,0:T(8,128)(2,1)S(1)} %collective-permute-done.4), channel_id=1, source_target_pairs={{0,4},{4,8},{8,12},{12,16},{16,20},{20,24},{24,28},{28,0},{1,5},{5... | collective-permute-start | bytes 393224 | tf_op jit(solution)/shard_map/ppermute | solution.py:21
Sparse Core Ops, SparseCore 0:
  15.3 71.5 reduce-scatter.1
  133.0 44.8 all-gather.1
